TPU v7x, 512 devices: a whole 4x4x16 slice. The times are simulated.
512 devices in a mesh: rep: 2 (over z_hi), fs: 32 (over z_lo, y), tp: 8 (over x, core).
Axes of the slice: x: 4, y: 4, z: 16 (z_hi: 2, z_lo: 8; z = z_hi * 8 + z_lo), core: 2. Of those that a mesh axis runs over, the one named last changes fastest.
Arguments:
- tokens_in: bfloat16 [16384, 2048], P(('rep', 'fs', 'tp')), may hold values from -6 to 6
- norm_gains: float32 [3, 2048], replicated, may hold values from 0.1 to 1.9
- gate_w: float32 [2048, 3072], P('fs', 'tp'), may hold values from -0.125 to 0.125
- gate_scale: float32 [3072], P('tp'), may hold values from 0.5 to 2
- up_w: float32 [2048, 3072], P('fs', 'tp'), may hold values from -0.125 to 0.125
- up_scale: float32 [3072], P('tp'), may hold values from 0.5 to 2
- down_w: float32 [3072, 2048], P('tp', 'fs'), may hold values from -0.109375 to 0.109375
- down_scale: float32 [2048], P('fs'), may hold values from 0.5 to 2
- query_w: float32 [2048, 2048], P('fs', 'tp'), may hold values from -0.125 to 0.125
- query_scale: float32 [2048], P('tp'), may hold values from 0.5 to 2
- key_w: float32 [2048, 2048], P('fs', 'tp'), may hold values from -0.125 to 0.125
- key_scale: float32 [2048], P('tp'), may hold values from 0.5 to 2
- value_w: float32 [2048, 2048], P('fs', 'tp'), may hold values from -0.125 to 0.125
- value_scale: float32 [2048], P('tp'), may hold values from 0.5 to 2
- out_w: float32 [2048, 2048], P('tp', 'fs'), may hold values from -0.125 to 0.125
- out_scale: float32 [2048], P('fs'), may hold values from 0.5 to 2
- head_gain: float32 [256], replicated, may hold values from 0.1 to 1.9
- decay_rate: float32 [8], P('tp'), may hold values from 0 to 1, as said below
Outputs:
- tokens_out: bfloat16 [16384, 2048], P(('rep', 'fs', 'tp'))
Inputs may be any that keep to these rules, and one draw needn't show every extreme that they name: `decay_rate`: each head's decay per position, positive.
All inputs are finite; a program needn't handle non-finite values.
Results may differ from a plain program's by a relative error of at most 0.02.
Values may be sent and summed in bfloat16 or wider, within the bound.
No kernel may reach another device: no remote copies, remote signals or barrier semaphores. Data moves between devices by JAX's collectives and lax.ppermute only.
A program may use at most 64 MiB of HBM per device.

v0:
```python
import math
import jax
import jax.numpy as jnp
from jax import lax
from jax.sharding import Mesh, PartitionSpec as P

DK = 256
DV = 256
BLOCK = 64
EPSILON = 1e-05


def gather_weights(packed):
    rep = lax.axis_index("rep")
    half = packed.shape[0] // 2
    mine = lax.dynamic_slice_in_dim(packed, rep * half, half, axis=0)
    full = lax.all_gather(mine, ("rep", "z", "y"), axis=0, tiled=True)
    return (
        full.reshape(2, -1, half, packed.shape[1])
        .transpose(1, 0, 2, 3)
        .reshape(-1, packed.shape[1])
    )


def norm_rows(stream, gain):
    scale = lax.rsqrt(jnp.mean(stream * stream, axis=-1, keepdims=True) + EPSILON)
    return (stream * scale * gain).astype(jnp.bfloat16)


def swap_cores(array):
    return lax.ppermute(array, "core", [(0, 1), (1, 0)])


def gather_rows(rows):
    n = lax.axis_size("x")
    copies = jnp.broadcast_to(rows, (n, *rows.shape))
    own = lax.all_to_all(copies, "x", split_axis=0, concat_axis=0, tiled=True)
    own = own.reshape(-1, rows.shape[1])
    return jnp.concatenate([own, swap_cores(own)], axis=0)


def return_rows(part):
    n = lax.axis_size("x")
    half = part.shape[0] // 2
    sent = swap_cores(part[half:].astype(jnp.bfloat16))
    both = (part[:half] + sent.astype(jnp.float32)).astype(jnp.bfloat16)
    blocks = both.reshape(n, half // n, -1)
    arrived = lax.all_to_all(blocks, "x", split_axis=0, concat_axis=0, tiled=True)
    return arrived.astype(jnp.float32).sum(axis=0)


def dot(a, b):
    return jnp.dot(a, b, preferred_element_type=jnp.float32)


def dot_t(a, b):
    return lax.dot_general(a, b, (((1,), (1,)), ((), ())), preferred_element_type=jnp.float32)


def positions(rows):
    n = lax.axis_size("x")
    core = lax.axis_index("core")
    r = jnp.arange(n * rows, dtype=jnp.int32)
    first = r // rows * (2 * rows) + r % rows
    return jnp.concatenate([first + core * rows, first + (1 - core) * rows])


def retain(query, key_rows, value, decay_rate, head_gain, pos):
    apart = jnp.abs(pos[:, None] - pos[None, :]).astype(jnp.float32)
    seen = pos[None, :] // BLOCK <= pos[:, None] // BLOCK
    decay = jnp.where(seen, jnp.exp(-decay_rate[0] * apart), 0.0)
    scores = (dot_t(query, key_rows) * decay).astype(jnp.bfloat16)
    retained = dot(scores, value)
    centred = retained - jnp.mean(retained, axis=-1, keepdims=True)
    scale = lax.rsqrt(jnp.mean(centred * centred, axis=-1, keepdims=True) + EPSILON)
    return (centred * scale * head_gain).astype(jnp.bfloat16)


def on_device(
    tokens_in,
    norm_gains,
    gate_w,
    gate_scale,
    up_w,
    up_scale,
    down_w,
    down_scale,
    query_w,
    query_scale,
    key_w,
    key_scale,
    value_w,
    value_scale,
    out_w,
    out_scale,
    head_gain,
    decay_rate,
):

    def low(w):
        return w.astype(jnp.bfloat16)

    down_t = low(low(down_w).T.astype(jnp.float32) * down_scale[:, None])
    out_t = low(low(out_w).T.astype(jnp.float32) * out_scale[:, None])
    pieces = [low(gate_w), low(up_w), down_t, low(query_w), low(key_w), low(value_w), out_t]
    packed = jnp.concatenate(pieces, axis=1)
    full = gather_weights(packed)
    at, parts = (0, [])
    for p in pieces:
        parts.append(full[:, at : at + p.shape[1]])
        at += p.shape[1]
    gate_f, up_f, down_f, query_f, key_f, value_f, out_f = parts

    def feed_forward(stream, gain):
        rows = gather_rows(norm_rows(stream, gain))
        gate = dot(rows, gate_f) * gate_scale
        up = dot(rows, up_f) * up_scale
        hidden = low(jax.nn.silu(gate) * up)
        return return_rows(dot_t(hidden, down_f))

    stream = tokens_in.astype(jnp.float32)
    stream = stream + 0.5 * feed_forward(stream, norm_gains[0])
    rows = gather_rows(norm_rows(stream, norm_gains[1]))
    query = low(dot(rows, query_f) * query_scale)
    key_rows = low(dot(rows, key_f) * key_scale / math.sqrt(DK))
    value = low(dot(rows, value_f) * value_scale)
    mixed = retain(query, key_rows, value, decay_rate, head_gain, positions(tokens_in.shape[0]))
    stream = stream + return_rows(dot_t(mixed, out_f))
    stream = stream + 0.5 * feed_forward(stream, norm_gains[2])
    return stream.astype(jnp.bfloat16)


def solution(mesh):
    devices = mesh.devices
    reps, fs, tp = devices.shape
    fine = Mesh(devices.reshape(reps, fs // 4, 4, tp // 2, 2), ("rep", "z", "y", "x", "core"))
    F, T = (("z", "y"), ("x", "core"))
    rows = P(("rep", "z", "y", "x", "core"), None)
    wide, tall, cols, depth = (P(F, T), P(T, F), P(T), P(F))
    placed = (
        rows,
        P(),
        wide,
        cols,
        wide,
        cols,
        tall,
        depth,
        wide,
        cols,
        wide,
        cols,
        wide,
        cols,
        tall,
        depth,
        P(),
        cols,
    )
    return jax.shard_map(on_device, mesh=fine, in_specs=placed, out_specs=rows, check_vma=False)
```

profile of v0, /device:TPU:1, one launch (start us, length us, event | category | flops | bytes accessed | tf_op | source)
XLA Modules:
  0.0 294.2 jit_solution(15299229404249725897)
XLA Ops:
  6.5 0.9 convert_dynamic-update-slice_fusion.1
  7.4 0.9 convert_dynamic-update-slice_fusion
  8.3 1.0 fusion.71
  9.3 0.8 convert_dynamic-update-slice_fusion.4
  10.2 0.8 convert_dynamic-update-slice_fusion.3
  11.0 0.8 convert_dynamic-update-slice_fusion.2
  11.9 0.9 fusion.73
  12.8 0.7 constant_dynamic-slice_fusion
  13.5 1.0 fusion.38
  14.6 0.9 fusion.89
  15.5 1.0 fusion.40
  16.5 11.6 %all_to_all.30 = bf16[4,32,2048]{2,1,0:T(8,128)(2,1)S(1)} all-to-all(bf16[4,32,2048]{2,1,0:T(8,128)(2,1)S(1)} %broadcast_in_dim.9), channel_id=1, replica_groups=mesh['rep'=2,'z'=8,'y'=4,'x'=4,'core'=2] {'x'}, dimensions={0} | all-to-all | bytes 1048576 | tf_op jit(solution)/shard_map/all_to_all | solution.py:37
  28.1 7.7 %collective-permute-start = (bf16[128,2048]{1,0:T(8,128)(2,1)S(1)}, bf16[128,2048]{1,0:T(8,128)(2,1)S(1)}, u32[]{:S(2)}, u32[]{:S(2)}) collective-permute-start(bf16[128,2048]{1,0:T(8,128)(2,1)S(1)} %bitcast.41), channel_id=1, source_target_pairs={{0,1},{1,0},{2,3},{3,2},{4,5},{5,4},{6,7},{7,6},{8,9},{9,8},{10,11... | collective-permute-start | bytes 1572872 | tf_op jit(solution)/shard_map/ppermute | solution.py:31
  35.8 133.1 %all-gather.2.cloned.1.call-done = bf16[2048,2176]{1,0:T(8,128)(2,1)} async-done(((bf16[32,2176]{1,0:T(8,128)(2,1)}), bf16[2048,2176]{1,0:T(8,128)(2,1)}) %all-gather.2.cloned.1.call-update) | async-done | bytes 8912912 | tf_op jit(solution)/shard_map/all_gather | solution.py:17
  168.9 8.2 %copy.19 = bf16[32,2,32,2176]{3,2,1,0:T(8,128)(2,1)} copy(bf16[32,2,32,2176]{3,2,0,1:T(8,128)(2,1)} %bitcast.33) | data formatting | bytes 17825792 | tf_op jit(solution)/shard_map/transpose | solution.py:20
  177.1 2.9 fusion.12
  180.1 3.4 %fusion.2 = f32[256,2048]{1,0:T(8,128)S(1)} fusion(bf16[2048,2176]{1,0:T(8,128)(2,1)} %bitcast.26, f32[256,384]{1,0:T(8,128)} %fusion.12, bf16[128,2048]{1,0:T(8,128)(2,1)S(1)} %collective-permute-done, bf16[128,2048]{1,0:T(8,128)(2,1)S(1)} %bitcast.43, f32[384]{0:T(512)S(1)} %copy-done.5), kind=kOutput, calls=%fused_computation.2 | convolution fusion | flops 808091648 | bytes 6686208 | tf_op jit(solution)/shard_map/dot_general | solution.py:57
  183.5 10.4 %collective-permute-start.1 = (bf16[128,2048]{1,0:T(8,128)(2,1)S(1)}, bf16[128,2048]{1,0:T(8,128)(2,1)S(1)}, u32[]{:S(2)}, u32[]{:S(2)}) collective-permute-start(bf16[128,2048]{1,0:T(8,128)(2,1)S(1)} %slice.130), channel_id=1, source_target_pairs={{0,1},{1,0},{2,3},{3,2},{4,5},{5,4},{6,7},{7,6},{8,9},{9,8},{10,11... | collective-permute-start | bytes 1572872 | tf_op jit(solution)/shard_map/ppermute | solution.py:31
  193.9 1.5 collective-permute-done.1
  195.4 0.1 fusion.37
  195.6 12.4 %all_to_all.31 = bf16[4,32,2048]{2,1,0:T(8,128)(2,1)S(1)} all-to-all(bf16[4,32,2048]{2,1,0:T(8,128)(2,1)S(1)} %bitcast.34), channel_id=1, replica_groups=mesh['rep'=2,'z'=8,'y'=4,'x'=4,'core'=2] {'x'}, dimensions={0} | all-to-all | bytes 1048576 | tf_op jit(solution)/shard_map/all_to_all | solution.py:48
  208.0 0.2 multiply_reduce_fusion.2
  208.2 0.1 multiply_convert_fusion.4
  208.3 10.2 %all_to_all.32 = bf16[4,32,2048]{2,1,0:T(8,128)(2,1)S(1)} all-to-all(bf16[4,32,2048]{2,1,0:T(8,128)(2,1)S(1)} %broadcast_in_dim.10), channel_id=1, replica_groups=mesh['rep'=2,'z'=8,'y'=4,'x'=4,'core'=2] {'x'}, dimensions={0} | all-to-all | bytes 1048576 | tf_op jit(solution)/shard_map/all_to_all | solution.py:37
  218.5 4.7 %collective-permute-start.2 = (bf16[128,2048]{1,0:T(8,128)(2,1)S(1)}, bf16[128,2048]{1,0:T(8,128)(2,1)S(1)}, u32[]{:S(2)}, u32[]{:S(2)}) collective-permute-start(bf16[128,2048]{1,0:T(8,128)(2,1)S(1)} %bitcast.37), channel_id=1, source_target_pairs={{0,1},{1,0},{2,3},{3,2},{4,5},{5,4},{6,7},{7,6},{8,9},{9,8},{10,11... | collective-permute-start | bytes 1572872 | tf_op jit(solution)/shard_map/ppermute | solution.py:31
  223.9 0.8 collective-permute-done.2
  224.7 1.7 fusion.26
  226.4 1.7 fusion.25
  228.1 1.7 fusion.27
  229.8 0.5 fusion.90
  230.3 1.8 fusion.32
  232.2 2.3 collective-permute-start.3
  234.5 1.5 collective-permute-done.3
  236.0 0.1 fusion.31
  236.1 11.6 %all_to_all.33 = bf16[4,32,2048]{2,1,0:T(8,128)(2,1)S(1)} all-to-all(bf16[4,32,2048]{2,1,0:T(8,128)(2,1)S(1)} %bitcast.35), channel_id=1, replica_groups=mesh['rep'=2,'z'=8,'y'=4,'x'=4,'core'=2] {'x'}, dimensions={0} | all-to-all | bytes 1048576 | tf_op jit(solution)/shard_map/all_to_all | solution.py:48
  247.8 0.2 multiply_reduce_fusion
  248.0 0.1 multiply_convert_fusion.2
  248.2 10.7 %all_to_all.34 = bf16[4,32,2048]{2,1,0:T(8,128)(2,1)S(1)} all-to-all(bf16[4,32,2048]{2,1,0:T(8,128)(2,1)S(1)} %broadcast_in_dim.12), channel_id=1, replica_groups=mesh['rep'=2,'z'=8,'y'=4,'x'=4,'core'=2] {'x'}, dimensions={0} | all-to-all | bytes 1048576 | tf_op jit(solution)/shard_map/all_to_all | solution.py:37
  258.9 4.1 %collective-permute-start.4 = (bf16[128,2048]{1,0:T(8,128)(2,1)S(1)}, bf16[128,2048]{1,0:T(8,128)(2,1)S(1)}, u32[]{:S(2)}, u32[]{:S(2)}) collective-permute-start(bf16[128,2048]{1,0:T(8,128)(2,1)S(1)} %bitcast.44), channel_id=1, source_target_pairs={{0,1},{1,0},{2,3},{3,2},{4,5},{5,4},{6,7},{7,6},{8,9},{9,8},{10,11... | collective-permute-start | bytes 1572872 | tf_op jit(solution)/shard_map/ppermute | solution.py:31
  263.0 1.5 collective-permute-done.4
  264.5 0.9 copy-done.2
  265.4 2.1 fusion.15
  267.6 3.4 %fusion = f32[256,2048]{1,0:T(8,128)S(1)} fusion(bf16[2048,2176]{1,0:T(8,128)(2,1)} %bitcast.32, f32[256,384]{1,0:T(8,128)S(1)} %fusion.15, bf16[128,2048]{1,0:T(8,128)(2,1)} %copy-done.2, bf16[128,2048]{1,0:T(8,128)(2,1)S(1)} %bitcast.46, f32[384]{0:T(512)S(1)} %copy-done.6), kind=kOutput, calls=%fused_computation | convolution fusion | flops 808091648 | bytes 6686208 | tf_op jit(solution)/shard_map/dot_general | solution.py:57
  271.0 2.3 collective-permute-start.5
  273.3 1.5 collective-permute-done.5
  274.9 0.1 fusion.30
  275.0 11.6 %all_to_all.35 = bf16[4,32,2048]{2,1,0:T(8,128)(2,1)S(1)} all-to-all(bf16[4,32,2048]{2,1,0:T(8,128)(2,1)S(1)} %bitcast.36), channel_id=1, replica_groups=mesh['rep'=2,'z'=8,'y'=4,'x'=4,'core'=2] {'x'}, dimensions={0} | all-to-all | bytes 1048576 | tf_op jit(solution)/shard_map/all_to_all | solution.py:48
  286.7 0.7 add_convert_fusion
  (39 shorter events, 0.7 us)
Async XLA Ops:
  6.5 162.3 %all-gather.2.cloned.1.call-start = ((), (), s32[]{:S(2)}) async-start(), calls=%async_computation.6 | async-start | bytes 9052160 | tf_op jit(solution)/shard_map/all_gather | solution.py:17
  28.1 149.0 %collective-permute-start = (bf16[128,2048]{1,0:T(8,128)(2,1)S(1)}, bf16[128,2048]{1,0:T(8,128)(2,1)S(1)}, u32[]{:S(2)}, u32[]{:S(2)}) collective-permute-start(bf16[128,2048]{1,0:T(8,128)(2,1)S(1)} %bitcast.41), channel_id=1, source_target_pairs={{0,1},{1,0},{2,3},{3,2},{4,5},{5,4},{6,7},{7,6},{8,9},{9,8},{10,11... | collective-permute-start | bytes 1572872 | tf_op jit(solution)/shard_map/ppermute | solution.py:31
  168.9 8.2 %copy-start.3 = (f32[384]{0:T(512)S(1)}, f32[384]{0:T(512)}, u32[]{:S(2)}) copy-start(f32[384]{0:T(512)} %param.21) | copy-start | bytes 4612
  177.1 2.9 %copy-start.5 = (f32[384]{0:T(512)S(1)}, f32[384]{0:T(512)}, u32[]{:S(2)}) copy-start(f32[384]{0:T(512)} %param.23) | copy-start | bytes 4612
  183.5 24.5 %copy-start = (bf16[32,2048]{1,0:T(8,128)(2,1)S(1)}, bf16[32,2048]{1,0:T(8,128)(2,1)}, u32[]{:S(2)}) copy-start(bf16[32,2048]{1,0:T(8,128)(2,1)} %param.18) | copy-start | bytes 393220
  183.5 11.9 %collective-permute-start.1 = (bf16[128,2048]{1,0:T(8,128)(2,1)S(1)}, bf16[128,2048]{1,0:T(8,128)(2,1)S(1)}, u32[]{:S(2)}, u32[]{:S(2)}) collective-permute-start(bf16[128,2048]{1,0:T(8,128)(2,1)S(1)} %slice.130), channel_id=1, source_target_pairs={{0,1},{1,0},{2,3},{3,2},{4,5},{5,4},{6,7},{7,6},{8,9},{9,8},{10,11... | collective-permute-start | bytes 1572872 | tf_op jit(solution)/shard_map/ppermute | solution.py:31
  195.5 29.2 %copy-start.7 = (f32[256]{0:T(256)S(1)}, f32[256]{0:T(256)}, u32[]{:S(2)}) copy-start(f32[256]{0:T(256)} %param.29) | copy-start | bytes 3076
  218.5 7.9 %copy-start.8 = (f32[256]{0:T(256)S(1)}, f32[256]{0:T(256)}, u32[]{:S(2)}) copy-start(f32[256]{0:T(256)} %param.27) | copy-start | bytes 3076
  218.5 6.2 %collective-permute-start.2 = (bf16[128,2048]{1,0:T(8,128)(2,1)S(1)}, bf16[128,2048]{1,0:T(8,128)(2,1)S(1)}, u32[]{:S(2)}, u32[]{:S(2)}) collective-permute-start(bf16[128,2048]{1,0:T(8,128)(2,1)S(1)} %bitcast.37), channel_id=1, source_target_pairs={{0,1},{1,0},{2,3},{3,2},{4,5},{5,4},{6,7},{7,6},{8,9},{9,8},{10,11... | collective-permute-start | bytes 1572872 | tf_op jit(solution)/shard_map/ppermute | solution.py:31
  226.4 1.7 copy-start.9
  228.1 2.2 copy-start.1
  232.2 3.8 %collective-permute-start.3 = (bf16[128,2048]{1,0:T(8,128)(2,1)S(1)}, bf16[128,2048]{1,0:T(8,128)(2,1)S(1)}, u32[]{:S(2)}, u32[]{:S(2)}) collective-permute-start(bf16[128,2048]{1,0:T(8,128)(2,1)S(1)} %slice.129), channel_id=1, source_target_pairs={{0,1},{1,0},{2,3},{3,2},{4,5},{5,4},{6,7},{7,6},{8,9},{9,8},{10,11... | collective-permute-start | bytes 1572872 | tf_op jit(solution)/shard_map/ppermute | solution.py:31
  247.7 17.7 %copy-start.4 = (f32[384]{0:T(512)S(1)}, f32[384]{0:T(512)}, u32[]{:S(2)}) copy-start(f32[384]{0:T(512)} %param.21) | copy-start | bytes 4612
  258.9 8.7 %copy-start.6 = (f32[384]{0:T(512)S(1)}, f32[384]{0:T(512)}, u32[]{:S(2)}) copy-start(f32[384]{0:T(512)} %param.23) | copy-start | bytes 4612
  258.9 5.6 %collective-permute-start.4 = (bf16[128,2048]{1,0:T(8,128)(2,1)S(1)}, bf16[128,2048]{1,0:T(8,128)(2,1)S(1)}, u32[]{:S(2)}, u32[]{:S(2)}) collective-permute-start(bf16[128,2048]{1,0:T(8,128)(2,1)S(1)} %bitcast.44), channel_id=1, source_target_pairs={{0,1},{1,0},{2,3},{3,2},{4,5},{5,4},{6,7},{7,6},{8,9},{9,8},{10,11... | collective-permute-start | bytes 1572872 | tf_op jit(solution)/shard_map/ppermute | solution.py:31
  264.5 0.9 copy-start.2
  271.0 3.8 %collective-permute-start.5 = (bf16[128,2048]{1,0:T(8,128)(2,1)S(1)}, bf16[128,2048]{1,0:T(8,128)(2,1)S(1)}, u32[]{:S(2)}, u32[]{:S(2)}) collective-permute-start(bf16[128,2048]{1,0:T(8,128)(2,1)S(1)} %slice.128), channel_id=1, source_target_pairs={{0,1},{1,0},{2,3},{3,2},{4,5},{5,4},{6,7},{7,6},{8,9},{9,8},{10,11... | collective-permute-start | bytes 1572872 | tf_op jit(solution)/shard_map/ppermute | solution.py:31
Sparse Core Ops, SparseCore 0:
  13.6 155.1 all-gather.1
where the time goes:
time: 295 us; the launch traced here: 294 us
  waiting for transfers between devices  140 us (47%)
  blocking collectives  68 us (23%)
  starting transfers between devices  31.4 us (11%)
  matrix products  19.1 us (6%)
  between operations  14.4 us (5%)
  local copies, waits for them, and re-layouts  11 us (4%)
  other arithmetic  10.2 us (3%)
    all_gather x1, waiting for transfers between devices, gather_weights(): full = lax.all_gather(mine, ('rep', 'z', 'y'), axis=0, tiled=True)  133 us
    all_to_all x3, blocking collectives, return_rows(): lax.all_to_all(blocks, 'x', split_axis=0, concat_axis=0, tiled=True)  35.6 us
    all_to_all x3, blocking collectives, gather_rows(): own = lax.all_to_all(copies, 'x', split_axis=0, concat_axis=0, tiled=True)  32.5 us
    ppermute x6, starting transfers between devices, swap_cores(): return lax.ppermute(array, 'core', [(0, 1), (1, 0)])  31.4 us
    dot_general x6, matrix products, dot(): return jnp.dot(a, b, preferred_element_type=jnp.float32)  10.5 us
    dot_general x3, matrix products, dot_t(): lax.dot_general(a, b, (((1,), (1,)), ((), ())), preferred_element_type=jn...  8.57 us
    transpose x1, local copies, waits for them, and re-layouts, gather_weights(): return full.reshape(2, -1, half, packed.shape[1]).transpose(1, 0, 2, 3).r...  8.24 us
    ppermute x6, waiting for transfers between devices, swap_cores(): return lax.ppermute(array, 'core', [(0, 1), (1, 0)])  6.89 us
  transfers between devices with their start and end apart: 7, of which 6 were waited for; matrix products, arithmetic and copies ran while one was open for 4% of the time, Pallas kernels for 0%

commit v1 on v0

--- a/solution.py
+++ b/solution.py
@@ -14,7 +14,8 @@
     rep = lax.axis_index("rep")
     half = packed.shape[0] // 2
     mine = lax.dynamic_slice_in_dim(packed, rep * half, half, axis=0)
-    full = lax.all_gather(mine, ("rep", "z", "y"), axis=0, tiled=True)
+    outgoing = jnp.stack([mine] * lax.axis_size(("rep", "z", "y")))
+    full = jnp.concatenate(lax.all_to_all(outgoing, ("rep", "z", "y"), 0, 0), axis=0)
     return (
         full.reshape(2, -1, half, packed.shape[1])
         .transpose(1, 0, 2, 3)

time: 295 us -> 543 us (1.84)
  waiting for transfers between devices: 140 us -> 393 us
  starting transfers between devices: 31.4 us -> 53.4 us
  between operations: 14.4 us -> 1.1 us
  blocking collectives: 68 us -> 56.3 us
  other arithmetic: 10.2 us -> 4.14 us
    all_to_all x0 -> x2, waiting for transfers between devices: none -> 386 us  [the longest x1 379 us: gather_weights(): lax.all_to_all(outgoing, ('rep', 'z', 'y'), 0, 0)]
    all_gather x1 -> x0, waiting for transfers between devices: 133 us -> none  [gather_weights(): full = lax.all_gather(mine, ('rep', 'z', 'y'), axis=0, tiled=True)]
    all_to_all x0 -> x2, starting transfers between devices: none -> 24.9 us  [the longest x1 20.1 us: gather_weights(): lax.all_to_all(outgoing, ('rep', 'z', 'y'), 0, 0)]
    all_to_all x3 -> x2, blocking collectives: 32.5 us -> 21.5 us  [gather_rows(): own = lax.all_to_all(copies, 'x', split_axis=0, concat_axis=0, tiled=True)]
  transfers between devices with their start and end apart: 7 -> 8, of which waited for: 6 -> 7; matrix products, arithmetic and copies ran while one was open for 4% -> 2% of each run, Pallas kernels for 0% -> 0%
where the time goes in v1:
time: 543 us; the launch traced here: 542 us
  waiting for transfers between devices  393 us (72%)
  blocking collectives  56.3 us (10%)
  starting transfers between devices  53.4 us (10%)
  matrix products  19.2 us (4%)
  local copies, waits for them, and re-layouts  15.3 us (3%)
    all_to_all x1, waiting for transfers between devices, gather_weights(): lax.all_to_all(outgoing, ('rep', 'z', 'y'), 0, 0)  379 us
    all_to_all x3, blocking collectives, return_rows(): lax.all_to_all(blocks, 'x', split_axis=0, concat_axis=0, tiled=True)  34.8 us
    ppermute x6, starting transfers between devices, swap_cores(): return lax.ppermute(array, 'core', [(0, 1), (1, 0)])  28.5 us
    all_to_all x2, blocking collectives, gather_rows(): own = lax.all_to_all(copies, 'x', split_axis=0, concat_axis=0, tiled=True)  21.5 us
    all_to_all x1, starting transfers between devices, gather_weights(): lax.all_to_all(outgoing, ('rep', 'z', 'y'), 0, 0)  20.1 us
  transfers between devices with their start and end apart: 8, of which 7 were waited for; matrix products, arithmetic and copies ran while one was open for 2% of the time, Pallas kernels for 0%

profile of v1, /device:TPU:1, one launch (start us, length us, event | category | flops | bytes accessed | tf_op | source)
XLA Modules:
  0.0 542.3 jit_solution(4056291673577262218)
XLA Ops:
  0.1 0.9 fusion.89
  1.0 1.0 fusion.38
  2.0 1.0 fusion.40
  3.1 0.9 broadcast_in_dim.9
  3.9 4.8 all-to-all-start
  8.8 0.1 fusion.71
  9.1 6.6 %all-to-all-done = bf16[4,32,2048]{2,1,0:T(8,128)(2,1)S(1)} async-done(((bf16[4,32,2048]{2,1,0:T(8,128)(2,1)}), bf16[4,32,2048]{2,1,0:T(8,128)(2,1)S(1)}, u32[]{:S(2)}, u32[]{:S(2)}) %all-to-all-start) | async-done | bytes 524320 | tf_op jit(solution)/shard_map/all_to_all | solution.py:38
  15.7 4.0 stack.2
  19.7 20.1 %all-to-all-start.1 = ((bf16[64,32,2176]{2,1,0:T(8,128)(2,1)}), bf16[64,32,2176]{2,1,0:T(8,128)(2,1)}, u32[]{:S(2)}, u32[]{:S(2)}) async-start(bf16[64,32,2176]{2,1,0:T(8,128)(2,1)} %stack.2), calls=%async_computation.1 | async-start | bytes 17825792 | tf_op jit(solution)/shard_map/all_to_all | solution.py:18
  39.8 4.3 collective-permute-start
  44.1 379.4 %all-to-all-done.1 = bf16[64,32,2176]{2,1,0:T(8,128)(2,1)} async-done(((bf16[64,32,2176]{2,1,0:T(8,128)(2,1)}), bf16[64,32,2176]{2,1,0:T(8,128)(2,1)}, u32[]{:S(2)}, u32[]{:S(2)}) %all-to-all-start.1) | async-done | bytes 8912928 | tf_op jit(solution)/shard_map/all_to_all | solution.py:18
  423.6 8.3 %copy.19 = bf16[32,2,32,2176]{3,2,1,0:T(8,128)(2,1)} copy(bf16[32,2,32,2176]{3,2,0,1:T(8,128)(2,1)} %bitcast.5) | data formatting | bytes 17825792 | tf_op jit(solution)/shard_map/transpose | solution.py:21
  431.8 2.9 fusion.12
  434.8 3.4 fusion.2
  438.2 11.5 %collective-permute-start.1 = (bf16[128,2048]{1,0:T(8,128)(2,1)S(1)}, bf16[128,2048]{1,0:T(8,128)(2,1)S(1)}, u32[]{:S(2)}, u32[]{:S(2)}) collective-permute-start(bf16[128,2048]{1,0:T(8,128)(2,1)S(1)} %slice.130), channel_id=1, source_target_pairs={{0,1},{1,0},{2,3},{3,2},{4,5},{5,4},{6,7},{7,6},{8,9},{9,8},{10,11... | collective-permute-start | bytes 1572872 | tf_op jit(solution)/shard_map/ppermute | solution.py:32
  449.8 1.5 collective-permute-done.1
  451.3 0.1 fusion.37
  451.4 11.6 %all_to_all.35 = bf16[4,32,2048]{2,1,0:T(8,128)(2,1)S(1)} all-to-all(bf16[4,32,2048]{2,1,0:T(8,128)(2,1)S(1)} %bitcast.33), channel_id=1, replica_groups=mesh['rep'=2,'z'=8,'y'=4,'x'=4,'core'=2] {'x'}, dimensions={0} | all-to-all | bytes 1048576 | tf_op jit(solution)/shard_map/all_to_all | solution.py:49
  463.0 0.1 convert_reduce_fusion.2
  463.1 0.2 multiply_reduce_fusion.2
  463.3 0.1 multiply_convert_fusion.4
  463.4 10.7 %all_to_all.36 = bf16[4,32,2048]{2,1,0:T(8,128)(2,1)S(1)} all-to-all(bf16[4,32,2048]{2,1,0:T(8,128)(2,1)S(1)} %broadcast_in_dim.10), channel_id=1, replica_groups=mesh['rep'=2,'z'=8,'y'=4,'x'=4,'core'=2] {'x'}, dimensions={0} | all-to-all | bytes 1048576 | tf_op jit(solution)/shard_map/all_to_all | solution.py:38
  474.2 4.1 collective-permute-start.2
  479.0 0.8 collective-permute-done.2
  479.8 1.7 fusion.26
  481.5 1.7 fusion.25
  483.3 1.7 fusion.27
  484.9 0.5 fusion.90
  485.5 1.8 fusion.32
  487.4 2.3 collective-permute-start.3
  489.7 1.5 collective-permute-done.3
  491.2 0.1 fusion.31
  491.3 11.6 %all_to_all.37 = bf16[4,32,2048]{2,1,0:T(8,128)(2,1)S(1)} all-to-all(bf16[4,32,2048]{2,1,0:T(8,128)(2,1)S(1)} %bitcast.34), channel_id=1, replica_groups=mesh['rep'=2,'z'=8,'y'=4,'x'=4,'core'=2] {'x'}, dimensions={0} | all-to-all | bytes 1048576 | tf_op jit(solution)/shard_map/all_to_all | solution.py:49
  502.9 0.1 convert_reduce_fusion.1
  503.0 0.2 multiply_reduce_fusion
  503.2 0.1 multiply_convert_fusion.2
  503.3 10.7 %all_to_all.38 = bf16[4,32,2048]{2,1,0:T(8,128)(2,1)S(1)} all-to-all(bf16[4,32,2048]{2,1,0:T(8,128)(2,1)S(1)} %broadcast_in_dim.12), channel_id=1, replica_groups=mesh['rep'=2,'z'=8,'y'=4,'x'=4,'core'=2] {'x'}, dimensions={0} | all-to-all | bytes 1048576 | tf_op jit(solution)/shard_map/all_to_all | solution.py:38
  514.1 4.0 collective-permute-start.4
  518.1 1.5 collective-permute-done.4
  519.6 0.8 copy-done.11
  520.4 2.1 fusion.15
  522.6 3.4 fusion
  526.0 2.3 collective-permute-start.5
  528.3 1.5 collective-permute-done.5
  529.8 0.1 fusion.30
  530.0 11.6 %all_to_all.39 = bf16[4,32,2048]{2,1,0:T(8,128)(2,1)S(1)} all-to-all(bf16[4,32,2048]{2,1,0:T(8,128)(2,1)S(1)} %bitcast.35), channel_id=1, replica_groups=mesh['rep'=2,'z'=8,'y'=4,'x'=4,'core'=2] {'x'}, dimensions={0} | all-to-all | bytes 1048576 | tf_op jit(solution)/shard_map/all_to_all | solution.py:49
  541.6 0.1 convert_reduce_fusion
  541.6 0.7 add_convert_fusion
  (54 shorter events, 0.6 us)
Async XLA Ops:
  0.0 8.8 %copy-start.1 = (f32[64,384]{1,0:T(8,128)S(1)}, f32[64,384]{1,0:T(8,128)}, u32[]{:S(2)}) copy-start(f32[64,384]{1,0:T(8,128)} %param.20) | copy-start | bytes 294916
  0.0 8.8 %copy-start.2 = (f32[64,384]{1,0:T(8,128)S(1)}, f32[64,384]{1,0:T(8,128)}, u32[]{:S(2)}) copy-start(f32[64,384]{1,0:T(8,128)} %param.22) | copy-start | bytes 294916
  0.0 8.8 %copy-start.3 = (f32[384,64]{0,1:T(8,128)S(1)}, f32[384,64]{0,1:T(8,128)}, u32[]{:S(2)}) copy-start(f32[384,64]{0,1:T(8,128)} %param.24) | copy-start | bytes 294916
  0.0 8.8 %copy-start.9 = (f32[64]{0:T(128)S(1)}, f32[64]{0:T(128)}, u32[]{:S(2)}) copy-start(f32[64]{0:T(128)} %param.25) | copy-start | bytes 772
  0.0 8.9 %copy-start.4 = (f32[64,256]{1,0:T(8,128)S(1)}, f32[64,256]{1,0:T(8,128)}, u32[]{:S(2)}) copy-start(f32[64,256]{1,0:T(8,128)} %param.26) | copy-start | bytes 196612
  0.0 8.9 %copy-start.5 = (f32[64,256]{1,0:T(8,128)S(1)}, f32[64,256]{1,0:T(8,128)}, u32[]{:S(2)}) copy-start(f32[64,256]{1,0:T(8,128)} %param.28) | copy-start | bytes 196612
  0.0 8.9 %copy-start.6 = (f32[64,256]{1,0:T(8,128)S(1)}, f32[64,256]{1,0:T(8,128)}, u32[]{:S(2)}) copy-start(f32[64,256]{1,0:T(8,128)} %param.30) | copy-start | bytes 196612
  0.0 8.9 %copy-start.7 = (f32[256,64]{0,1:T(8,128)S(1)}, f32[256,64]{0,1:T(8,128)}, u32[]{:S(2)}) copy-start(f32[256,64]{0,1:T(8,128)} %param.32) | copy-start | bytes 196612
  0.1 8.9 %copy-start.10 = (f32[64]{0:T(128)S(1)}, f32[64]{0:T(128)}, u32[]{:S(2)}) copy-start(f32[64]{0:T(128)} %param.33) | copy-start | bytes 772
  3.9 11.8 %all-to-all-start = ((bf16[4,32,2048]{2,1,0:T(8,128)(2,1)}), bf16[4,32,2048]{2,1,0:T(8,128)(2,1)S(1)}, u32[]{:S(2)}, u32[]{:S(2)}) async-start(bf16[4,32,2048]{2,1,0:T(8,128)(2,1)} %broadcast_in_dim.9), calls=%async_computation | async-start | bytes 1048576 | tf_op jit(solution)/shard_map/all_to_all | solution.py:38
  19.7 403.8 %all-to-all-start.1 = ((bf16[64,32,2176]{2,1,0:T(8,128)(2,1)}), bf16[64,32,2176]{2,1,0:T(8,128)(2,1)}, u32[]{:S(2)}, u32[]{:S(2)}) async-start(bf16[64,32,2176]{2,1,0:T(8,128)(2,1)} %stack.2), calls=%async_computation.1 | async-start | bytes 17825792 | tf_op jit(solution)/shard_map/all_to_all | solution.py:18
  39.8 392.0 %collective-permute-start = (bf16[128,2048]{1,0:T(8,128)(2,1)S(1)}, bf16[128,2048]{1,0:T(8,128)(2,1)S(1)}, u32[]{:S(2)}, u32[]{:S(2)}) collective-permute-start(bf16[128,2048]{1,0:T(8,128)(2,1)S(1)} %bitcast.36), channel_id=1, source_target_pairs={{0,1},{1,0},{2,3},{3,2},{4,5},{5,4},{6,7},{7,6},{8,9},{9,8},{10,11... | collective-permute-start | bytes 1572872 | tf_op jit(solution)/shard_map/ppermute | solution.py:32
  423.6 8.3 %copy-start.12 = (f32[384]{0:T(512)S(1)}, f32[384]{0:T(512)}, u32[]{:S(2)}) copy-start(f32[384]{0:T(512)} %param.21) | copy-start | bytes 4612
  431.8 2.9 copy-start.13
  438.2 24.9 %copy-start = (bf16[32,2048]{1,0:T(8,128)(2,1)S(1)}, bf16[32,2048]{1,0:T(8,128)(2,1)}, u32[]{:S(2)}) copy-start(bf16[32,2048]{1,0:T(8,128)(2,1)} %param.18) | copy-start | bytes 393220
  438.2 13.0 %collective-permute-start.1 = (bf16[128,2048]{1,0:T(8,128)(2,1)S(1)}, bf16[128,2048]{1,0:T(8,128)(2,1)S(1)}, u32[]{:S(2)}, u32[]{:S(2)}) collective-permute-start(bf16[128,2048]{1,0:T(8,128)(2,1)S(1)} %slice.130), channel_id=1, source_target_pairs={{0,1},{1,0},{2,3},{3,2},{4,5},{5,4},{6,7},{7,6},{8,9},{9,8},{10,11... | collective-permute-start | bytes 1572872 | tf_op jit(solution)/shard_map/ppermute | solution.py:32
  451.4 28.4 %copy-start.14 = (f32[256]{0:T(256)S(1)}, f32[256]{0:T(256)}, u32[]{:S(2)}) copy-start(f32[256]{0:T(256)} %param.29) | copy-start | bytes 3076
  474.2 7.4 %copy-start.15 = (f32[256]{0:T(256)S(1)}, f32[256]{0:T(256)}, u32[]{:S(2)}) copy-start(f32[256]{0:T(256)} %param.27) | copy-start | bytes 3076
  474.2 5.6 %collective-permute-start.2 = (bf16[128,2048]{1,0:T(8,128)(2,1)S(1)}, bf16[128,2048]{1,0:T(8,128)(2,1)S(1)}, u32[]{:S(2)}, u32[]{:S(2)}) collective-permute-start(bf16[128,2048]{1,0:T(8,128)(2,1)S(1)} %bitcast.39), channel_id=1, source_target_pairs={{0,1},{1,0},{2,3},{3,2},{4,5},{5,4},{6,7},{7,6},{8,9},{9,8},{10,11... | collective-permute-start | bytes 1572872 | tf_op jit(solution)/shard_map/ppermute | solution.py:32
  481.5 1.7 copy-start.16
  483.2 2.2 copy-start.8
  487.4 3.8 collective-permute-start.3
  514.1 5.5 %collective-permute-start.4 = (bf16[128,2048]{1,0:T(8,128)(2,1)S(1)}, bf16[128,2048]{1,0:T(8,128)(2,1)S(1)}, u32[]{:S(2)}, u32[]{:S(2)}) collective-permute-start(bf16[128,2048]{1,0:T(8,128)(2,1)S(1)} %bitcast.43), channel_id=1, source_target_pairs={{0,1},{1,0},{2,3},{3,2},{4,5},{5,4},{6,7},{7,6},{8,9},{9,8},{10,11... | collective-permute-start | bytes 1572872 | tf_op jit(solution)/shard_map/ppermute | solution.py:32
  519.6 0.8 copy-start.11
  526.0 3.8 collective-permute-start.5
